TPU v7x, 512 devices: a whole 4x8x8 slice. The times are simulated.
512 devices in a mesh: fs: 128 (over z, y, core), tp: 4 (over x).
Axes of the slice: x: 4, y: 8, z: 8, core: 2. Of those that a mesh axis runs over, the one named last changes fastest.
Arguments:
- rnn_out: bfloat16 [98304, 1536], P('fs', 'tp'), may hold values from -6 to 6
- out_grad: bfloat16 [98304, 2048], P('fs', 'tp'), may hold values from -0.078125 to 0.078125
- weight: float32 [2048, 1536], P('fs', 'tp'), may hold values from -0.15625 to 0.15625
- left_root: bfloat16 [4, 2048, 2048], P('tp', 'fs'), as said below
- right_root: bfloat16 [4, 384, 384], P('tp'), as said below
- left_stat: float32 [4, 2048, 2048], P('tp', 'fs'), may hold values from -4 to 4
- right_stat: float32 [4, 384, 384], P('tp', 'fs'), may hold values from -4 to 4
Outputs:
- new_weight: float32 [2048, 1536], P('fs', 'tp')
- step: float32 [2048, 1536], P('fs', 'tp')
- left_new: float32 [4, 2048, 2048], P('tp', 'fs')
- right_new: float32 [4, 384, 384], P('tp', 'fs')
- weight_copy: bfloat16 [2048, 1536], P(None, 'tp')
Inputs may be any that keep to these rules, and one draw needn't show every extreme that they name: `left_root`: each block is symmetric. `right_root`: each block is symmetric.
All inputs are finite; a program needn't handle non-finite values.
Results may differ from a plain program's by a relative error of at most 0.0049.
Values may be sent and summed in bfloat16 or wider, within the bound.
A program may use at most 64 MiB of HBM per device.

v0:
```python
import jax
import jax.numpy as jnp
from jax import lax
from jax.sharding import Mesh
from jax.sharding import PartitionSpec as P

FS = ("fs_0", "fs_1", "fs_2")
FS_TP = ("fs_0", "fs_1", "fs_2", "tp")
decay_rate = 0.8
step_size = 0.005


def by_axis(shard, axes):
    for axis in axes:
        shard = lax.psum(shard, axis)
    return shard


def laid_out(pieces, dim):
    shape = list(pieces.shape[1:])
    shape[dim] *= pieces.shape[0]
    return jnp.moveaxis(pieces, 0, dim).reshape(shape)


def stacked_from(shard, axes, turns):
    pieces = shard[None]
    for k in turns:
        pieces = lax.all_gather(pieces, axes[k], axis=0, tiled=True)
    current = [lax.axis_size(axes[k]) for k in reversed(turns)]
    pieces = pieces.reshape(*current, *shard.shape)
    turned = sorted(range(len(turns)), key=lambda place: turns[len(turns) - 1 - place])
    return pieces.transpose(*turned, *range(len(turns), pieces.ndim)).reshape(-1, *shard.shape)


def gathered_by_axis(shard, axes, turns, dim):
    return laid_out(stacked_from(shard, axes, turns), dim)


def body(rnn_out, out_grad, weight, left_root, right_root, left_stat, right_stat):
    row_count = weight.shape[0]
    block = weight.shape[1]
    width = left_root.shape[2]
    right_rows = right_stat.shape[1]
    right_start = lax.axis_index(FS) * right_rows
    cotangent = lax.all_gather(out_grad, "tp", axis=1, tiled=True)
    whole = lax.psum(
        lax.dot_general(
            cotangent, rnn_out, (((0,), (0,)), ((), ())), preferred_element_type=jnp.float32
        ),
        FS,
    )
    whole_low = whole.astype(jnp.bfloat16)
    grad = lax.dynamic_slice_in_dim(whole, lax.axis_index(FS) * row_count, row_count, 0)
    grad_low = grad.astype(jnp.bfloat16)
    root_columns = left_root[0]
    left_sum = jnp.dot(root_columns, whole_low, preferred_element_type=jnp.float32)
    own_columns = lax.dynamic_slice_in_dim(whole_low, right_start, right_rows, 1)
    right_sum = lax.dot_general(
        own_columns, whole_low, (((0,), (0,)), ((), ())), preferred_element_type=jnp.float32
    )
    product = lax.dot_general(
        grad_low, whole_low, (((1,), (1,)), ((), ())), preferred_element_type=jnp.float32
    )
    outer = product
    left_sum, right_sum, outer = (left_sum, right_sum, outer)
    grad_square = jnp.sum(grad * grad)
    left_new = decay_rate * left_stat + (1.0 - decay_rate) * (outer / block)[None]
    right_new = decay_rate * right_stat + (1.0 - decay_rate) * (right_sum / width)[None]
    applied = left_sum.astype(jnp.bfloat16)
    update = jnp.dot(applied, right_root[0], preferred_element_type=jnp.float32)
    update_square = jnp.sum(update * update)
    total_grad, total_update = (by_axis(grad_square, FS_TP), by_axis(update_square, FS_TP))
    scale = jnp.sqrt(total_grad + 1.0) / jnp.sqrt(total_update + 1.0)
    step = scale * update
    new_weight = weight - step_size * step
    weight_copy = gathered_by_axis(new_weight.astype(jnp.bfloat16), FS, (0, 1, 2), 0)
    return (new_weight, step, left_new, right_new, weight_copy)


def solution(mesh):
    torus = Mesh(mesh.devices.reshape(8, 8, 2, mesh.shape["tp"]), ("fs_0", "fs_1", "fs_2", "tp"))
    return jax.shard_map(
        body,
        mesh=torus,
        in_specs=(
            P(FS, "tp"),
            P(FS, "tp"),
            P(FS, "tp"),
            P("tp", FS, None),
            P("tp", None, None),
            P("tp", FS, None),
            P("tp", FS, None),
        ),
        out_specs=(P(FS, "tp"), P(FS, "tp"), P("tp", FS, None), P("tp", FS, None), P(None, "tp")),
        check_vma=False,
    )
```

profile of v0, /device:TPU:1, one launch (start us, length us, event | category | flops | bytes accessed | tf_op | source)
XLA Modules:
  0.0 400.5 jit_solution(8813950215224952123)
XLA Ops:
  7.2 0.0 copy-start
  7.2 0.0 all-gather.4.cloned.1.call-start
  7.2 0.7 all-gather.4.cloned.1.call-update
  7.9 0.0 all-reduce.6.cloned.1.call-start
  8.0 52.3 %all-gather.4.cloned.1.call-done = bf16[768,2048]{1,0:T(8,128)(2,1)} async-done(((bf16[768,512]{1,0:T(8,128)(2,1)}), bf16[768,2048]{1,0:T(8,128)(2,1)}) %all-gather.4.cloned.1.call-update) | async-done | bytes 3145744 | tf_op jit(solution)/shard_map/all_gather | solution.py:45
  60.2 0.0 copy-done
  60.2 5.4 %fusion.14 = f32[2048,384]{1,0:T(8,128)} fusion(bf16[768,2048]{1,0:T(8,128)(2,1)} %all-gather.4.cloned.1.call-done, bf16[768,384]{1,0:T(8,128)(2,1)S(1)} %copy-done), kind=kOutput, calls=%fused_computation.20 | convolution fusion | flops 1207959552 | bytes 6881280 | tf_op jit(solution)/shard_map/dot_general | solution.py:47
  65.7 0.0 all-reduce.6.cloned.1.call-update
  65.7 0.0 all-gather.6.cloned.1.call-start
  65.8 0.0 copy-start.4
  65.8 0.0 copy-start.5
  65.8 203.9 %all-reduce.6.cloned.1.call-done = f32[2048,384]{1,0:T(8,128)} async-done(((f32[2048,384]{1,0:T(8,128)}), f32[2048,384]{1,0:T(8,128)}) %all-reduce.6.cloned.1.call-update) | async-done | bytes 3145744 | tf_op jit(solution)/shard_map/psum | solution.py:46
  269.7 2.1 convert_element_type.13
  271.8 0.0 copy-done.4
  271.8 0.0 copy-done.5
  271.8 0.0 copy-start.2
  271.8 0.0 copy-start.3
  271.8 1.4 multiply_reduce_fusion
  273.2 1.3 multiply_reduce_fusion.1
  274.6 13.3 %all-reduce.1 = (f32[]{:T(128)}, f32[]{:T(128)}) all-reduce(f32[]{:T(128)} %multiply_reduce_fusion.1, f32[]{:T(128)} %get-tuple-element.26), channel_id=1, replica_groups=mesh['fs_0'=8,'fs_1'=8,'fs_2'=2,'tp'=4] {'fs_0'}, use_global_device_ids=true, to_apply=%region_2.0 | all-reduce | flops 2 | bytes 16 | tf_op jit(solution)/shard_map/psum | solution.py:15
  287.8 14.7 %all-reduce = (f32[]{:T(128)}, f32[]{:T(128)}) all-reduce(f32[]{:T(128)} %get-tuple-element.17, f32[]{:T(128)} %get-tuple-element.18), channel_id=1, replica_groups=mesh['fs_0'=8,'fs_1'=8,'fs_2'=2,'tp'=4] {'fs_1'}, use_global_device_ids=true, to_apply=%region_3.0 | all-reduce | flops 2 | bytes 16 | tf_op jit(solution)/shard_map/psum | solution.py:15
  302.6 9.2 %all-reduce.3 = (f32[]{:T(128)}, f32[]{:T(128)}) all-reduce(f32[]{:T(128)} %get-tuple-element.15, f32[]{:T(128)} %get-tuple-element.16), channel_id=1, replica_groups=mesh['fs_0'=8,'fs_1'=8,'fs_2'=2,'tp'=4] {'fs_2'}, use_global_device_ids=true, to_apply=%region_4.0 | all-reduce | flops 2 | bytes 16 | tf_op jit(solution)/shard_map/psum | solution.py:15
  311.8 9.0 %all-reduce.2 = (f32[]{:T(128)}, f32[]{:T(128)}) all-reduce(f32[]{:T(128)} %get-tuple-element.21, f32[]{:T(128)} %get-tuple-element.22), channel_id=1, replica_groups=mesh['fs_0'=8,'fs_1'=8,'fs_2'=2,'tp'=4] {'tp'}, use_global_device_ids=true, to_apply=%region_5.0 | all-reduce | flops 2 | bytes 16 | tf_op jit(solution)/shard_map/psum | solution.py:15
  322.1 0.0 copy-done.2
  322.2 0.6 fusion.11
  322.8 18.5 %all-gather = bf16[128,384]{1,0:T(8,128)(2,1)S(1)} all-gather(bf16[16,384]{1,0:T(8,128)(2,1)S(1)} %get-tuple-element.23), channel_id=2, replica_groups=mesh['fs_0'=8,'fs_1'=8,'fs_2'=2,'tp'=4] {'fs_0'}, dimensions={0}, use_global_device_ids=true | all-gather | bytes 110592 | tf_op jit(solution)/shard_map/all_gather | solution.py:28
  341.3 0.0 copy-start.1
  341.3 22.1 %all_gather.14 = bf16[64,16,384]{2,1,0:T(8,128)(2,1)} all-gather(bf16[8,16,384]{2,1,0:T(8,128)(2,1)S(1)} %bitcast.31), channel_id=1, replica_groups=mesh['fs_0'=8,'fs_1'=8,'fs_2'=2,'tp'=4] {'fs_1'}, dimensions={0}, use_global_device_ids=true | all-gather | bytes 884736 | tf_op jit(solution)/shard_map/all_gather | solution.py:28
  363.4 0.0 all-gather.6.cloned.1.call-update
  363.5 0.0 copy-done.3
  363.5 0.6 fusion.4
  364.1 0.6 copy.17
  364.7 0.0 copy-done.1
  364.7 1.9 fusion.1
  366.6 24.6 %all-gather.6.cloned.1.call-done = bf16[128,16,384]{2,1,0:T(8,128)(2,1)} async-done(((bf16[64,16,384]{2,1,0:T(8,128)(2,1)}), bf16[128,16,384]{2,1,0:T(8,128)(2,1)}) %all-gather.6.cloned.1.call-update) | async-done | bytes 1572880 | tf_op jit(solution)/shard_map/all_gather | solution.py:28
  391.3 2.7 copy.16
Async XLA Ops:
  7.2 53.1 %copy-start = (bf16[768,384]{1,0:T(8,128)(2,1)S(1)}, bf16[768,384]{1,0:T(8,128)(2,1)}, u32[]{:S(2)}) copy-start(bf16[768,384]{1,0:T(8,128)(2,1)} %param.7) | copy-start | bytes 1769476
  7.2 53.1 %all-gather.4.cloned.1.call-start = ((), (), s32[]{:S(2)}) async-start(), calls=%async_computation | async-start | bytes 3932160 | tf_op jit(solution)/shard_map/all_gather | solution.py:45
  7.9 261.8 %all-reduce.6.cloned.1.call-start = ((), (), s32[]{:S(2)}) async-start(), calls=%async_computation.1 | async-start | bytes 6291456 | tf_op jit(solution)/shard_map/psum | solution.py:46
  65.7 325.6 %all-gather.6.cloned.1.call-start = ((), (), s32[]{:S(2)}) async-start(), calls=%async_computation.2 | async-start | bytes 2359296 | tf_op jit(solution)/shard_map/all_gather | solution.py:28
  65.8 206.0 %copy-start.4 = (bf16[1,384,384]{2,1,0:T(8,128)(2,1)S(1)}, bf16[1,384,384]{2,1,0:T(8,128)(2,1)}, u32[]{:S(2)}) copy-start(bf16[1,384,384]{2,1,0:T(8,128)(2,1)} %param.11) | copy-start | bytes 884740
  65.8 206.0 %copy-start.5 = (bf16[1,16,2048]{2,1,0:T(8,128)(2,1)S(1)}, bf16[1,16,2048]{2,1,0:T(8,128)(2,1)}, u32[]{:S(2)}) copy-start(bf16[1,16,2048]{2,1,0:T(8,128)(2,1)} %param.10) | copy-start | bytes 196612
  271.8 50.4 %copy-start.2 = (f32[16,384]{1,0:T(8,128)S(1)}, f32[16,384]{1,0:T(8,128)}, u32[]{:S(2)}) copy-start(f32[16,384]{1,0:T(8,128)} %param.9) | copy-start | bytes 73732
  271.8 91.7 %copy-start.3 = (f32[1,3,384]{2,0,1:T(1,128)S(1)}, f32[1,3,384]{2,0,1:T(1,128)}, u32[]{:S(2)}) copy-start(f32[1,3,384]{2,0,1:T(1,128)} %param.13) | copy-start | bytes 13828
  341.3 23.4 %copy-start.1 = (f32[1,16,2048]{2,1,0:T(8,128)S(1)}, f32[1,16,2048]{2,1,0:T(8,128)}, u32[]{:S(2)}) copy-start(f32[1,16,2048]{2,1,0:T(8,128)} %param.12) | copy-start | bytes 393220
Sparse Core Ops, SparseCore 0:
  10.1 50.1 all-gather.3
  65.8 203.8 all-reduce.5
  363.6 27.6 all-gather.5
where the time goes:
time: 401 us
  waiting for transfers between devices  282 us (70%)
  blocking collectives  86.9 us (22%)
  between operations  15.2 us (4%)
  matrix products  9.37 us (2%)
  other arithmetic  4.03 us (1%)
    psum x1, waiting for transfers between devices, body(): lax.psum(lax.dot_general(cotangent, rnn_out, (((0,), (0,)), ((), ())), pr...  204 us
    all_gather x1, waiting for transfers between devices, body(): cotangent = lax.all_gather(out_grad, 'tp', axis=1, tiled=True)  52.3 us
    psum x4, blocking collectives, by_axis(): shard = lax.psum(shard, axis)  46.2 us
    all_gather x2, blocking collectives, stacked_from(): pieces = lax.all_gather(pieces, axes[k], axis=0, tiled=True)  40.7 us
    all_gather x1, waiting for transfers between devices, stacked_from(): pieces = lax.all_gather(pieces, axes[k], axis=0, tiled=True)  24.6 us
  transfers between devices with their start and end apart: 3, of which 3 were waited for; matrix products, arithmetic and copies ran while one was open for 1% of the time, Pallas kernels for 0%

commit v1 on v0

--- a/solution.py
+++ b/solution.py
@@ -12,7 +12,7 @@
 
 def by_axis(shard, axes):
     for axis in axes:
-        shard = lax.psum(shard, axis)
+        shard = jnp.sum(lax.all_gather(shard, axis), axis=0)
     return shard
 
 

time: 401 us -> 418 us (1.042)
  local copies, waits for them, and re-layouts: 3.4 us -> 19.7 us
  other arithmetic: 4.03 us -> 8.84 us
    psum x4 -> x0, blocking collectives: 46.2 us -> none  [by_axis(): shard = lax.psum(shard, axis)]
    unnamed x0 -> x4, blocking collectives: none -> 43.6 us
    unnamed x13 -> x33, local copies, waits for them, and re-layouts: 0.65 us -> 16.9 us
    reduce_sum x0 -> x8, other arithmetic: none -> 4.81 us  [by_axis(): shard = jnp.sum(lax.all_gather(shard, axis), axis=0)]
where the time goes in v1:
time: 418 us
  waiting for transfers between devices  280 us (67%)
  blocking collectives  84.3 us (20%)
  local copies, waits for them, and re-layouts  19.7 us (5%)
  between operations  15.2 us (4%)
  matrix products  9.37 us (2%)
  other arithmetic  8.84 us (2%)
    psum x1, waiting for transfers between devices, body(): lax.psum(lax.dot_general(cotangent, rnn_out, (((0,), (0,)), ((), ())), pr...  203 us
    all_gather x1, waiting for transfers between devices, body(): cotangent = lax.all_gather(out_grad, 'tp', axis=1, tiled=True)  52.3 us
    unnamed x4, blocking collectives  43.6 us
    all_gather x2, blocking collectives, stacked_from(): pieces = lax.all_gather(pieces, axes[k], axis=0, tiled=True)  40.7 us
    all_gather x1, waiting for transfers between devices, stacked_from(): pieces = lax.all_gather(pieces, axes[k], axis=0, tiled=True)  24.6 us
    unnamed x33, local copies, waits for them, and re-layouts  16.9 us
  transfers between devices with their start and end apart: 3, of which 3 were waited for; matrix products, arithmetic and copies ran while one was open for 1% of the time, Pallas kernels for 0%

profile of v1, /device:TPU:1, one launch (start us, length us, event | category | flops | bytes accessed | tf_op | source)
XLA Modules:
  0.0 417.8 jit_solution(1842948748651501969)
XLA Ops:
  7.2 0.0 copy-start
  7.2 0.0 all-gather.4.cloned.1.call-start
  7.2 0.7 all-gather.4.cloned.1.call-update
  7.9 0.0 all-reduce.14.cloned.1.call-start
  8.0 52.3 %all-gather.4.cloned.1.call-done = bf16[768,2048]{1,0:T(8,128)(2,1)} async-done(((bf16[768,512]{1,0:T(8,128)(2,1)}), bf16[768,2048]{1,0:T(8,128)(2,1)}) %all-gather.4.cloned.1.call-update) | async-done | bytes 3145744 | tf_op jit(solution)/shard_map/all_gather | solution.py:45
  60.2 0.0 copy-done
  60.2 5.4 %fusion.14 = f32[2048,384]{1,0:T(8,128)} fusion(bf16[768,2048]{1,0:T(8,128)(2,1)} %all-gather.4.cloned.1.call-done, bf16[768,384]{1,0:T(8,128)(2,1)S(1)} %copy-done), kind=kOutput, calls=%fused_computation.20 | convolution fusion | flops 1207959552 | bytes 6881280 | tf_op jit(solution)/shard_map/dot_general | solution.py:47
  65.7 0.0 all-reduce.14.cloned.1.call-update
  65.7 0.0 all-gather.6.cloned.1.call-start
  65.8 1.3 dynamic-slice
  67.0 202.7 %all-reduce.14.cloned.1.call-done = f32[2048,384]{1,0:T(8,128)} async-done(((f32[2048,384]{1,0:T(8,128)}), f32[2048,384]{1,0:T(8,128)}) %all-reduce.14.cloned.1.call-update) | async-done | bytes 3145744 | tf_op jit(solution)/shard_map/psum | solution.py:46
  269.7 2.1 convert_element_type.13
  271.8 0.0 copy-start.2
  271.8 0.0 copy-start.3
  271.8 1.4 multiply_reduce_fusion
  273.2 1.3 multiply_reduce_fusion.1
  274.5 1.4 dynamic-update-slice
  275.9 1.4 dynamic-update-slice.4
  277.3 1.3 dynamic-slice.1
  278.6 12.6 %all-reduce.9 = (f32[8]{0:T(128)S(1)}, f32[8]{0:T(128)S(1)}) all-reduce(f32[8]{0:T(128)S(1)} %dynamic-update-slice, f32[8]{0:T(128)S(1)} %dynamic-update-slice.4), channel_id=1, replica_groups=mesh['fs_0'=8,'fs_1'=8,'fs_2'=2,'tp'=4] {'fs_0'}, use_global_device_ids=true, to_apply=%add | all-reduce | flops 16 | bytes 128
  291.2 0.6 reduce_sum.91
  291.8 0.6 reduce_sum.96
  292.4 1.4 dynamic-update-slice.1
  293.8 1.4 dynamic-update-slice.5
  295.2 1.3 dynamic-slice.2
  296.5 14.1 %all-reduce.8 = (f32[8]{0:T(128)S(1)}, f32[8]{0:T(128)S(1)}) all-reduce(f32[8]{0:T(128)S(1)} %dynamic-update-slice.1, f32[8]{0:T(128)S(1)} %dynamic-update-slice.5), channel_id=1, replica_groups=mesh['fs_0'=8,'fs_1'=8,'fs_2'=2,'tp'=4] {'fs_1'}, use_global_device_ids=true, to_apply=%add.1 | all-reduce | flops 16 | bytes 128
  310.6 0.6 reduce_sum.92
  311.2 0.6 reduce_sum.97
  311.8 1.4 dynamic-update-slice.2
  313.2 1.4 dynamic-update-slice.6
  314.6 1.3 dynamic-slice.3
  315.9 8.5 %all-reduce.11 = (f32[2]{0:T(128)S(1)}, f32[2]{0:T(128)S(1)}) all-reduce(f32[2]{0:T(128)S(1)} %dynamic-update-slice.2, f32[2]{0:T(128)S(1)} %dynamic-update-slice.6), channel_id=1, replica_groups=mesh['fs_0'=8,'fs_1'=8,'fs_2'=2,'tp'=4] {'fs_2'}, use_global_device_ids=true, to_apply=%add.2 | all-reduce | flops 4 | bytes 32
  324.4 0.6 reduce_sum.93
  325.0 0.6 reduce_sum.98
  325.6 1.4 dynamic-update-slice.3
  327.0 1.4 dynamic-update-slice.7
  328.4 8.4 %all-reduce.10 = (f32[4]{0:T(128)S(1)}, f32[4]{0:T(128)S(1)}) all-reduce(f32[4]{0:T(128)S(1)} %dynamic-update-slice.3, f32[4]{0:T(128)S(1)} %dynamic-update-slice.7), channel_id=1, replica_groups=mesh['fs_0'=8,'fs_1'=8,'fs_2'=2,'tp'=4] {'tp'}, use_global_device_ids=true, to_apply=%add.3 | all-reduce | flops 8 | bytes 64
  336.8 0.6 reduce_sum.94
  338.1 0.6 reduce_sum.99
  339.4 0.6 fusion.11
  340.0 18.5 %all-gather = bf16[128,384]{1,0:T(8,128)(2,1)S(1)} all-gather(bf16[16,384]{1,0:T(8,128)(2,1)S(1)} %get-tuple-element.23), channel_id=2, replica_groups=mesh['fs_0'=8,'fs_1'=8,'fs_2'=2,'tp'=4] {'fs_0'}, dimensions={0}, use_global_device_ids=true | all-gather | bytes 110592 | tf_op jit(solution)/shard_map/all_gather | solution.py:28
  358.6 22.1 %all_gather.78 = bf16[64,16,384]{2,1,0:T(8,128)(2,1)} all-gather(bf16[8,16,384]{2,1,0:T(8,128)(2,1)S(1)} %bitcast.43), channel_id=1, replica_groups=mesh['fs_0'=8,'fs_1'=8,'fs_2'=2,'tp'=4] {'fs_1'}, dimensions={0}, use_global_device_ids=true | all-gather | bytes 884736 | tf_op jit(solution)/shard_map/all_gather | solution.py:28
  380.7 0.0 all-gather.6.cloned.1.call-update
  380.7 0.6 fusion.4
  381.4 0.6 copy.17
  382.0 1.9 fusion.1
  383.9 24.6 %all-gather.6.cloned.1.call-done = bf16[128,16,384]{2,1,0:T(8,128)(2,1)} async-done(((bf16[64,16,384]{2,1,0:T(8,128)(2,1)}), bf16[128,16,384]{2,1,0:T(8,128)(2,1)}) %all-gather.6.cloned.1.call-update) | async-done | bytes 1572880 | tf_op jit(solution)/shard_map/all_gather | solution.py:28
  408.5 2.7 copy.16
  (16 shorter events, 0.0 us)
Async XLA Ops:
  7.2 53.1 %copy-start = (bf16[768,384]{1,0:T(8,128)(2,1)S(1)}, bf16[768,384]{1,0:T(8,128)(2,1)}, u32[]{:S(2)}) copy-start(bf16[768,384]{1,0:T(8,128)(2,1)} %param.7) | copy-start | bytes 1769476
  7.2 53.1 %all-gather.4.cloned.1.call-start = ((), (), s32[]{:S(2)}) async-start(), calls=%async_computation | async-start | bytes 3932160 | tf_op jit(solution)/shard_map/all_gather | solution.py:45
  7.9 261.8 %all-reduce.14.cloned.1.call-start = ((), (), s32[]{:S(2)}) async-start(), calls=%async_computation.1 | async-start | bytes 6291456 | tf_op jit(solution)/shard_map/psum | solution.py:46
  65.7 342.8 %all-gather.6.cloned.1.call-start = ((), (), s32[]{:S(2)}) async-start(), calls=%async_computation.2 | async-start | bytes 2359296 | tf_op jit(solution)/shard_map/all_gather | solution.py:28
  67.0 204.7 %copy-start.4 = (bf16[1,384,384]{2,1,0:T(8,128)(2,1)S(1)}, bf16[1,384,384]{2,1,0:T(8,128)(2,1)}, u32[]{:S(2)}) copy-start(bf16[1,384,384]{2,1,0:T(8,128)(2,1)} %param.11) | copy-start | bytes 884740
  67.0 204.7 %copy-start.5 = (bf16[1,16,2048]{2,1,0:T(8,128)(2,1)S(1)}, bf16[1,16,2048]{2,1,0:T(8,128)(2,1)}, u32[]{:S(2)}) copy-start(bf16[1,16,2048]{2,1,0:T(8,128)(2,1)} %param.10) | copy-start | bytes 196612
  271.8 67.6 %copy-start.2 = (f32[16,384]{1,0:T(8,128)S(1)}, f32[16,384]{1,0:T(8,128)}, u32[]{:S(2)}) copy-start(f32[16,384]{1,0:T(8,128)} %param.9) | copy-start | bytes 73732
  271.8 109.0 %copy-start.3 = (f32[1,3,384]{2,0,1:T(1,128)S(1)}, f32[1,3,384]{2,0,1:T(1,128)}, u32[]{:S(2)}) copy-start(f32[1,3,384]{2,0,1:T(1,128)} %param.13) | copy-start | bytes 13828
  358.6 23.4 %copy-start.1 = (f32[1,16,2048]{2,1,0:T(8,128)S(1)}, f32[1,16,2048]{2,1,0:T(8,128)}, u32[]{:S(2)}) copy-start(f32[1,16,2048]{2,1,0:T(8,128)} %param.12) | copy-start | bytes 393220
Sparse Core Ops, SparseCore 0:
  10.1 50.1 all-gather.3
  65.8 203.8 all-reduce.13
  380.8 27.6 all-gather.5
